TPU v7x, 32 devices: a whole 2x2x4 slice. The times are simulated.
32 devices in a mesh: grp: 2 (over x), sp: 4 (over y, core), tp: 4 (over z).
Axes of the slice: x: 2, y: 2, z: 4, core: 2. Of those that a mesh axis runs over, the one named last changes fastest.
Arguments:
- layer_input: bfloat16 [8, 1024, 2048], P(('grp', 'tp'), 'sp'), parts along dimension 0, may hold values from -6 to 6
- norm_gain: bfloat16 [2048], replicated, may hold values from 0.099609375 to 1.8984375
- key_weight: bfloat16 [2048, 1024], replicated, may hold values from -0.125 to 0.125
- value_weight: bfloat16 [2048, 1024], replicated, may hold values from -0.125 to 0.125
- input_gate_weight: bfloat16 [2048, 8], replicated, may hold values from -0.125 to 0.125
- forget_gate_weight: bfloat16 [2048, 8], replicated, may hold values from -0.125 to 0.125
- conv_weight: float32 [4, 1024], replicated, may hold values from -3 to 3
- input_shift: float32 [8, 8, 1024], P(('grp', 'sp'), 'tp'), parts along dimension 0, may hold values from -4 to 302
- forget_shift: float32 [8, 8, 1024], P(('grp', 'sp'), 'tp'), parts along dimension 0, may hold values from 0 to 10.1
- new_query: bfloat16 [8, 8, 128], P(('grp', 'sp'), 'tp'), parts along dimension 0, may hold values from 0.1 to 2
- new_key: bfloat16 [8, 8, 128], P(('grp', 'sp'), 'tp'), parts along dimension 0, may hold values from -6 to 6
- new_value: bfloat16 [8, 8, 128], P(('grp', 'sp'), 'tp'), parts along dimension 0, may hold values from -6 to 6
- new_input: float32 [8, 8], P(('grp', 'sp'), 'tp'), parts along dimension 0, may hold values from 2 to 6
- new_forget: float32 [8, 8], P(('grp', 'sp'), 'tp'), parts along dimension 0, may hold values from -1 to 3
Outputs:
- key_cache: bfloat16 [8, 8, 1024, 128], P(('grp', 'sp'), 'tp'), parts along dimension 0
- value_cache: bfloat16 [8, 8, 1024, 128], P(('grp', 'sp'), 'tp'), parts along dimension 0
- weight_cache: float32 [8, 8, 1024], P(('grp', 'sp'), 'tp'), parts along dimension 0
- first_read: bfloat16 [8, 8, 128], P(('grp', 'sp'), 'tp'), parts along dimension 0
There are 2 independent parts, one for each index of `grp`. A program takes and returns all parts, laid end to end along the dimension named above; an argument that names none is the same for every part. Nothing has to cross between parts.
All inputs are finite; a program needn't handle non-finite values.
Results may differ from a plain program's by a relative error of at most 0.012.
Values may be sent and summed in bfloat16 or wider, within the bound.
A program may use at most 64 MiB of HBM per device.

v0:
```python
import jax
import jax.numpy as jnp
from jax import lax
from jax.sharding import PartitionSpec as P

HEADS = 8
DK = 128
CONV = 4
epsilon = 1e-06


def shifted(block, axis, distance):
    devices = range(lax.axis_size(axis))
    route = [(i - distance, i) for i in devices if i - distance in devices]
    return lax.ppermute(block, axis, route)


def project_rows(
    token_rows, norm_gain, key_weight, value_weight, input_gate_weight, forget_gate_weight
):
    widened = token_rows.astype(jnp.float32)
    normed = (
        widened
        * lax.rsqrt(jnp.mean(widened * widened, axis=-1, keepdims=True) + epsilon)
        * norm_gain.astype(jnp.float32)
    ).astype(jnp.bfloat16)
    key_matrix = key_weight.reshape(key_weight.shape[0], HEADS, DK)
    value_matrix = value_weight.reshape(value_weight.shape[0], HEADS, DK)
    key_linear = jnp.einsum(
        "apd,dhk->ahpk", normed, key_matrix, preferred_element_type=jnp.float32
    ).astype(jnp.bfloat16)
    values = jnp.einsum(
        "apd,dhk->ahpk", normed, value_matrix, preferred_element_type=jnp.float32
    ).astype(jnp.bfloat16)
    input_linear = jnp.einsum(
        "apd,dh->ahp", normed, input_gate_weight, preferred_element_type=jnp.float32
    ).astype(jnp.bfloat16)
    forget_linear = jnp.einsum(
        "apd,dh->ahp", normed, forget_gate_weight, preferred_element_type=jnp.float32
    ).astype(jnp.bfloat16)
    return (key_linear, values, input_linear, forget_linear)


def convolve(key_linear, previous, conv_weight):
    extended = jnp.concatenate([previous, key_linear], axis=2).astype(jnp.float32)
    length = key_linear.shape[2]
    tap_weight = conv_weight.reshape(CONV, HEADS, 1, DK)
    summed = extended[:, :, 0:length, :] * tap_weight[0]
    for offset in range(1, CONV):
        summed = summed + extended[:, :, offset : offset + length, :] * tap_weight[offset]
    return jax.nn.silu(summed).astype(jnp.bfloat16)


def read_cache(
    keys,
    values,
    input_linear,
    forget_linear,
    input_shift,
    forget_shift,
    new_query,
    new_key,
    new_value,
    new_input,
    new_forget,
):
    scaling = DK ** (-0.5)
    log_forget = jax.nn.log_sigmoid(forget_linear.astype(jnp.float32) + forget_shift)
    suffix = lax.cumsum(log_forget, axis=2, reverse=True) - log_forget
    new_decay = jax.nn.log_sigmoid(new_forget)
    log_weight = input_linear.astype(jnp.float32) + input_shift + suffix + new_decay[:, :, None]
    largest = jnp.maximum(jnp.max(log_weight, axis=2), new_input)
    weight_cache = jnp.exp(log_weight - largest[:, :, None])
    new_weight = jnp.exp(new_input - largest)
    matched = jnp.einsum("bhlk,bhk->bhl", keys, new_query, preferred_element_type=jnp.float32)
    scores = (weight_cache * matched * scaling).astype(jnp.bfloat16)
    fresh_match = jnp.sum(new_key.astype(jnp.float32) * new_query.astype(jnp.float32), axis=2)
    new_score = (new_weight * fresh_match * scaling).astype(jnp.bfloat16)
    denominator = jnp.sum(scores.astype(jnp.float32), axis=2) + new_score.astype(jnp.float32)
    numerator = jnp.einsum("bhl,bhlk->bhk", scores, values, preferred_element_type=jnp.float32)
    numerator = numerator + new_score.astype(jnp.float32)[:, :, None] * new_value.astype(
        jnp.float32
    )
    first_read = (numerator / jnp.maximum(jnp.abs(denominator), 1.0)[:, :, None]).astype(
        jnp.bfloat16
    )
    return (weight_cache, first_read)


def shards(
    layer_input,
    norm_gain,
    key_weight,
    value_weight,
    input_gate_weight,
    forget_gate_weight,
    conv_weight,
    input_shift,
    forget_shift,
    new_query,
    new_key,
    new_value,
    new_input,
    new_forget,
):
    key_linear, values, input_linear, forget_linear = project_rows(
        layer_input, norm_gain, key_weight, value_weight, input_gate_weight, forget_gate_weight
    )
    previous = shifted(key_linear[:, :, -(CONV - 1) :, :], "sp", 1)
    keys = convolve(key_linear, previous, conv_weight)
    keys, values, input_linear, forget_linear = (
        lax.all_to_all(
            lax.all_to_all(keys, "tp", split_axis=1, concat_axis=0, tiled=True),
            "sp",
            split_axis=0,
            concat_axis=2,
            tiled=True,
        ),
        lax.all_to_all(
            lax.all_to_all(values, "tp", split_axis=1, concat_axis=0, tiled=True),
            "sp",
            split_axis=0,
            concat_axis=2,
            tiled=True,
        ),
        lax.all_to_all(
            lax.all_to_all(input_linear, "tp", split_axis=1, concat_axis=0, tiled=True),
            "sp",
            split_axis=0,
            concat_axis=2,
            tiled=True,
        ),
        lax.all_to_all(
            lax.all_to_all(forget_linear, "tp", split_axis=1, concat_axis=0, tiled=True),
            "sp",
            split_axis=0,
            concat_axis=2,
            tiled=True,
        ),
    )
    weight_cache, first_read = read_cache(
        keys,
        values,
        input_linear,
        forget_linear,
        input_shift,
        forget_shift,
        new_query,
        new_key,
        new_value,
        new_input,
        new_forget,
    )
    return (keys, values, weight_cache, first_read)


def solution(mesh):
    in_specs = (
        P(("grp", "tp"), "sp", None),
        P(),
        P(),
        P(),
        P(),
        P(),
        P(),
        P(("grp", "sp"), "tp", None),
        P(("grp", "sp"), "tp", None),
        P(("grp", "sp"), "tp", None),
        P(("grp", "sp"), "tp", None),
        P(("grp", "sp"), "tp", None),
        P(("grp", "sp"), "tp"),
        P(("grp", "sp"), "tp"),
    )
    out_specs = (
        P(("grp", "sp"), "tp", None, None),
        P(("grp", "sp"), "tp", None, None),
        P(("grp", "sp"), "tp", None),
        P(("grp", "sp"), "tp", None),
    )
    return jax.shard_map(shards, mesh=mesh, in_specs=in_specs, out_specs=out_specs, check_vma=False)
```

profile of v0, /device:TPU:0, one launch (start us, length us, event | category | flops | bytes accessed | tf_op | source)
XLA Modules:
  0.0 106.6 jit_solution(14466072062410166473)
XLA Ops:
  0.6 0.0 copy-start
  0.7 0.8 convert_element_type.131
  1.4 1.5 %fusion.6 = f32[256]{0:T(256)S(1)} fusion(bf16[1,256,2048]{2,1,0:T(8,128)(2,1)} %param.14), kind=kLoop, calls=%fused_computation.8 | loop fusion | flops 1572608 | bytes 1049600 | tf_op jit(solution)/shard_map/reduce_sum | solution.py:24
  3.0 1.7 %fusion.22 = bf16[1,8,256]{2,1,0:T(8,128)(2,1)S(1)} fusion(bf16[2048,8]{0,1:T(8,128)(2,1)S(1)} %copy-done, bf16[1,256,2048]{2,1,0:T(8,128)(2,1)} %param.14, f32[2048]{0:T(1024)S(1)} %convert_element_type.131, f32[256]{0:T(256)S(1)} %add_rsqrt_fusion), kind=kOutput, calls=%fused_computation.18 | convolution fusion | flops 10487808 | bytes 1094656 | tf_op jit(solution)/shard_map/apd,dh->ahp/dot_general | solution.py:38
  4.7 0.5 broadcast.50
  5.2 0.7 reduce.10
  5.9 0.6 reshape.225
  6.5 6.3 %all-to-all-start.6 = ((bf16[4,2,256]{2,1,0:T(2,128)(2,1)}), bf16[4,2,256]{2,1,0:T(2,128)(2,1)S(1)}, u32[]{:S(2)}, u32[]{:S(2)}) async-start(bf16[4,2,256]{2,1,0:T(2,128)(2,1)} %reshape.225), calls=%async_computation.6 | async-start | bytes 8192 | tf_op jit(solution)/shard_map/all_to_all | solution.py:134
  12.8 0.4 fusion.21
  13.3 0.7 reduce.11
  14.0 0.6 reshape.227
  14.6 3.8 %all-to-all-done.6 = bf16[4,2,256]{2,1,0:T(2,128)(2,1)S(1)} async-done(((bf16[4,2,256]{2,1,0:T(2,128)(2,1)}), bf16[4,2,256]{2,1,0:T(2,128)(2,1)S(1)}, u32[]{:S(2)}, u32[]{:S(2)}) %all-to-all-start.6) | async-done | bytes 4128 | tf_op jit(solution)/shard_map/all_to_all | solution.py:134
  18.4 3.2 %all-to-all-start.4 = ((bf16[4,2,256]{2,1,0:T(2,128)(2,1)}), bf16[4,2,256]{2,1,0:T(2,128)(2,1)S(1)}, u32[]{:S(2)}, u32[]{:S(2)}) async-start(bf16[4,2,256]{2,1,0:T(2,128)(2,1)} %reshape.227), calls=%async_computation.4 | async-start | bytes 8192 | tf_op jit(solution)/shard_map/all_to_all | solution.py:127
  21.7 0.6 all_to_all.92
  22.3 4.9 %all-to-all-done.4 = bf16[4,2,256]{2,1,0:T(2,128)(2,1)S(1)} async-done(((bf16[4,2,256]{2,1,0:T(2,128)(2,1)}), bf16[4,2,256]{2,1,0:T(2,128)(2,1)S(1)}, u32[]{:S(2)}, u32[]{:S(2)}) %all-to-all-start.4) | async-done | bytes 4128 | tf_op jit(solution)/shard_map/all_to_all | solution.py:127
  27.2 3.2 %all-to-all-start.7 = ((bf16[4,2,256]{2,1,0:T(2,128)(2,1)}), bf16[4,2,256]{2,1,0:T(2,128)(2,1)S(1)}, u32[]{:S(2)}, u32[]{:S(2)}) async-start(bf16[4,2,256]{2,1,0:T(2,128)(2,1)} %all_to_all.92), calls=%async_computation.7 | async-start | bytes 8192 | tf_op jit(solution)/shard_map/all_to_all | solution.py:133
  30.5 0.6 all_to_all.89
  31.1 3.1 %all-to-all-done.7 = bf16[4,2,256]{2,1,0:T(2,128)(2,1)S(1)} async-done(((bf16[4,2,256]{2,1,0:T(2,128)(2,1)}), bf16[4,2,256]{2,1,0:T(2,128)(2,1)S(1)}, u32[]{:S(2)}, u32[]{:S(2)}) %all-to-all-start.7) | async-done | bytes 4128 | tf_op jit(solution)/shard_map/all_to_all | solution.py:133
  34.2 3.2 %all-to-all-start.5 = ((bf16[4,2,256]{2,1,0:T(2,128)(2,1)}), bf16[4,2,256]{2,1,0:T(2,128)(2,1)S(1)}, u32[]{:S(2)}, u32[]{:S(2)}) async-start(bf16[4,2,256]{2,1,0:T(2,128)(2,1)} %all_to_all.89), calls=%async_computation.5 | async-start | bytes 8192 | tf_op jit(solution)/shard_map/all_to_all | solution.py:126
  37.5 4.3 %fusion.15 = bf16[1,8,256,128]{3,2,0,1:T(8,128)(2,1)} fusion(bf16[1,256,2048]{2,1,0:T(8,128)(2,1)S(1)} %copy-done.3, f32[2048]{0:T(1024)S(1)} %convert_element_type.131, f32[256]{0:T(256)S(1)} %add_rsqrt_fusion, bf16[2048,1024]{1,0:T(8,128)(2,1)} %param.17), kind=kOutput, calls=%fused_computation.13 | convolution fusion | flops 1076101120 | bytes 5776384 | tf_op jit(solution)/shard_map/apd,dhk->ahpk/dot_general | solution.py:32
  41.8 4.1 %all-to-all-start.2 = ((bf16[1,8,256,128]{3,2,0,1:T(8,128)(2,1)}), bf16[1,8,256,128]{3,2,0,1:T(8,128)(2,1)}, u32[]{:S(2)}, u32[]{:S(2)}) async-start(bf16[1,8,256,128]{3,2,0,1:T(8,128)(2,1)} %fusion.15), calls=%async_computation.2 | async-start | bytes 1048576 | tf_op jit(solution)/shard_map/all_to_all | solution.py:120
  45.9 3.5 %fusion.18 = bf16[1,8,256,128]{3,2,1,0:T(8,128)(2,1)S(1)} fusion(bf16[1,256,2048]{2,1,0:T(8,128)(2,1)S(1)} %copy-done.3, f32[2048]{0:T(1024)S(1)} %convert_element_type.131, f32[256]{0:T(256)S(1)} %add_rsqrt_fusion, bf16[2048,1024]{1,0:T(8,128)(2,1)} %param.16), kind=kOutput, calls=%fused_computation.14 | convolution fusion | flops 1076101120 | bytes 5776384 | tf_op jit(solution)/shard_map/apd,dhk->ahpk/dot_general | solution.py:29
  49.4 2.4 %collective-permute-start = (bf16[1,8,3,128]{3,2,1,0:T(4,128)(2,1)S(1)}, bf16[1,8,3,128]{3,2,1,0:T(4,128)(2,1)S(1)}, u32[]{:S(2)}, u32[]{:S(2)}) collective-permute-start(bf16[1,8,3,128]{3,2,1,0:T(4,128)(2,1)S(1)} %slice.48), channel_id=1, source_target_pairs={{0,4},{4,8},{8,12},{1,5},{5,9},{9,13},{2,6},{6,10},{10,14},{3,7},{... | collective-permute-start | bytes 18440 | tf_op jit(solution)/shard_map/ppermute | solution.py:15
  51.8 0.8 collective-permute-done
  52.6 0.1 maximum_convert_fusion
  52.7 0.0 copy-start.11
  52.8 0.0 copy-start.12
  52.8 1.5 %fusion.30 = bf16[1,8,256,128]{3,2,0,1:T(8,128)(2,1)} fusion(f32[8,128]{1,0:T(8,128)S(1)} %bitcast.172, f32[1,8,259,128]{3,2,1,0:T(8,128)S(1)} %maximum_convert_fusion, f32[8,128]{1,0:T(8,128)S(1)} %bitcast.173, f32[8,128]{1,0:T(8,128)S(1)} %bitcast.171, f32[8,128]{1,0:T(8,128)S(1)} %bitcast.170), kind=kLoop, calls=%fused_computation.32 | loop fusion | flops 3145728 | bytes 4734976 | tf_op jit(solution)/shard_map/convert_element_type | solution.py:51
  54.2 7.1 %all-to-all-done.2 = bf16[1,8,256,128]{3,2,0,1:T(8,128)(2,1)} async-done(((bf16[1,8,256,128]{3,2,0,1:T(8,128)(2,1)}), bf16[1,8,256,128]{3,2,0,1:T(8,128)(2,1)}, u32[]{:S(2)}, u32[]{:S(2)}) %all-to-all-start.2) | async-done | bytes 524320 | tf_op jit(solution)/shard_map/all_to_all | solution.py:120
  61.4 4.1 %all-to-all-start = ((bf16[1,8,256,128]{3,2,0,1:T(8,128)(2,1)}), bf16[1,8,256,128]{3,2,0,1:T(8,128)(2,1)}, u32[]{:S(2)}, u32[]{:S(2)}) async-start(bf16[1,8,256,128]{3,2,0,1:T(8,128)(2,1)} %fusion.30), calls=%async_computation | async-start | bytes 1048576 | tf_op jit(solution)/shard_map/all_to_all | solution.py:113
  65.5 0.1 multiply_reduce_fusion
  65.7 2.5 %reduce-window.6 = f32[1,2,8,128]{3,2,1,0:T(8,128)S(1)} reduce-window(f32[1,2,8,128]{3,2,1,0:T(8,128)S(1)} %copy.82, f32[]{:T(128)} %constant.7.clone.1), window={size=1x1x1x128 pad=0_0x0_0x0_0x0_127}, to_apply=%region_1.2 | reduce-window | flops 260096 | bytes 16388 | tf_op jit(solution)/shard_map/reduce-window
  68.2 0.1 slice_reduce_fusion
  68.3 0.2 reduce-window.9
  68.5 11.6 %all-to-all-done = bf16[1,8,256,128]{3,2,0,1:T(8,128)(2,1)} async-done(((bf16[1,8,256,128]{3,2,0,1:T(8,128)(2,1)}), bf16[1,8,256,128]{3,2,0,1:T(8,128)(2,1)}, u32[]{:S(2)}, u32[]{:S(2)}) %all-to-all-start) | async-done | bytes 524320 | tf_op jit(solution)/shard_map/all_to_all | solution.py:113
  80.1 3.5 %all-to-all-start.3 = ((bf16[4,2,256,128]{3,2,1,0:T(8,128)(2,1)}), bf16[4,2,256,128]{3,2,1,0:T(8,128)(2,1)S(1)}, u32[]{:S(2)}, u32[]{:S(2)}) async-start(bf16[4,2,256,128]{3,2,1,0:T(8,128)(2,1)} %bitcast.18), calls=%async_computation.3 | async-start | bytes 1048576 | tf_op jit(solution)/shard_map/all_to_all | solution.py:119
  83.6 0.1 slice_bitcast_fusion
  83.6 0.1 broadcast.41
  83.7 8.6 %all-to-all-done.3 = bf16[4,2,256,128]{3,2,1,0:T(8,128)(2,1)S(1)} async-done(((bf16[4,2,256,128]{3,2,1,0:T(8,128)(2,1)}), bf16[4,2,256,128]{3,2,1,0:T(8,128)(2,1)S(1)}, u32[]{:S(2)}, u32[]{:S(2)}) %all-to-all-start.3) | async-done | bytes 524320 | tf_op jit(solution)/shard_map/all_to_all | solution.py:119
  92.3 3.6 %all-to-all-start.1 = ((bf16[4,2,256,128]{3,2,1,0:T(8,128)(2,1)}), bf16[4,2,256,128]{3,2,1,0:T(8,128)(2,1)S(1)}, u32[]{:S(2)}, u32[]{:S(2)}) async-start(bf16[4,2,256,128]{3,2,1,0:T(8,128)(2,1)} %bitcast.10), calls=%async_computation.1 | async-start | bytes 1048576 | tf_op jit(solution)/shard_map/all_to_all | solution.py:112
  96.0 0.2 fusion.55
  96.2 0.0 copy-start.1
  96.2 8.5 %all-to-all-done.1 = bf16[4,2,256,128]{3,2,1,0:T(8,128)(2,1)S(1)} async-done(((bf16[4,2,256,128]{3,2,1,0:T(8,128)(2,1)}), bf16[4,2,256,128]{3,2,1,0:T(8,128)(2,1)S(1)}, u32[]{:S(2)}, u32[]{:S(2)}) %all-to-all-start.1) | async-done | bytes 524320 | tf_op jit(solution)/shard_map/all_to_all | solution.py:112
  104.8 0.0 copy-start.2
  104.8 0.2 fusion.36
  105.0 0.8 convert_reduce_fusion
  105.8 0.2 fusion.34
  106.0 0.6 fusion.38
  (42 shorter events, 0.4 us)
Async XLA Ops:
  0.6 2.3 %copy-start = (bf16[2048,8]{0,1:T(8,128)(2,1)S(1)}, bf16[2048,8]{0,1:T(8,128)(2,1)}, u32[]{:S(2)}) copy-start(bf16[2048,8]{0,1:T(8,128)(2,1)} %param.19) | copy-start | bytes 98308
  0.6 12.2 %copy-start.3 = (bf16[1,256,2048]{2,1,0:T(8,128)(2,1)S(1)}, bf16[1,256,2048]{2,1,0:T(8,128)(2,1)}, u32[]{:S(2)}) copy-start(bf16[1,256,2048]{2,1,0:T(8,128)(2,1)} %param.14) | copy-start | bytes 3145732
  0.7 12.2 %copy-start.10 = (bf16[2048,8]{0,1:T(8,128)(2,1)S(1)}, bf16[2048,8]{0,1:T(8,128)(2,1)}, u32[]{:S(2)}) copy-start(bf16[2048,8]{0,1:T(8,128)(2,1)} %param.18) | copy-start | bytes 98308
  6.5 11.9 %all-to-all-start.6 = ((bf16[4,2,256]{2,1,0:T(2,128)(2,1)}), bf16[4,2,256]{2,1,0:T(2,128)(2,1)S(1)}, u32[]{:S(2)}, u32[]{:S(2)}) async-start(bf16[4,2,256]{2,1,0:T(2,128)(2,1)} %reshape.225), calls=%async_computation.6 | async-start | bytes 8192 | tf_op jit(solution)/shard_map/all_to_all | solution.py:134
  18.4 8.8 %all-to-all-start.4 = ((bf16[4,2,256]{2,1,0:T(2,128)(2,1)}), bf16[4,2,256]{2,1,0:T(2,128)(2,1)S(1)}, u32[]{:S(2)}, u32[]{:S(2)}) async-start(bf16[4,2,256]{2,1,0:T(2,128)(2,1)} %reshape.227), calls=%async_computation.4 | async-start | bytes 8192 | tf_op jit(solution)/shard_map/all_to_all | solution.py:127
  27.2 7.0 %all-to-all-start.7 = ((bf16[4,2,256]{2,1,0:T(2,128)(2,1)}), bf16[4,2,256]{2,1,0:T(2,128)(2,1)S(1)}, u32[]{:S(2)}, u32[]{:S(2)}) async-start(bf16[4,2,256]{2,1,0:T(2,128)(2,1)} %all_to_all.92), calls=%async_computation.7 | async-start | bytes 8192 | tf_op jit(solution)/shard_map/all_to_all | solution.py:133
  34.2 7.5 %all-to-all-start.5 = ((bf16[4,2,256]{2,1,0:T(2,128)(2,1)}), bf16[4,2,256]{2,1,0:T(2,128)(2,1)S(1)}, u32[]{:S(2)}, u32[]{:S(2)}) async-start(bf16[4,2,256]{2,1,0:T(2,128)(2,1)} %all_to_all.89), calls=%async_computation.5 | async-start | bytes 8192 | tf_op jit(solution)/shard_map/all_to_all | solution.py:126
  41.8 19.6 %all-to-all-start.2 = ((bf16[1,8,256,128]{3,2,0,1:T(8,128)(2,1)}), bf16[1,8,256,128]{3,2,0,1:T(8,128)(2,1)}, u32[]{:S(2)}, u32[]{:S(2)}) async-start(bf16[1,8,256,128]{3,2,0,1:T(8,128)(2,1)} %fusion.15), calls=%async_computation.2 | async-start | bytes 1048576 | tf_op jit(solution)/shard_map/all_to_all | solution.py:120
  45.9 5.9 %copy-start.5 = (f32[4,1024]{1,0:T(4,128)S(1)}, f32[4,1024]{1,0:T(4,128)}, u32[]{:S(2)}) copy-start(f32[4,1024]{1,0:T(4,128)} %param.20) | copy-start | bytes 49156
  49.4 3.2 %collective-permute-start = (bf16[1,8,3,128]{3,2,1,0:T(4,128)(2,1)S(1)}, bf16[1,8,3,128]{3,2,1,0:T(4,128)(2,1)S(1)}, u32[]{:S(2)}, u32[]{:S(2)}) collective-permute-start(bf16[1,8,3,128]{3,2,1,0:T(4,128)(2,1)S(1)} %slice.48), channel_id=1, source_target_pairs={{0,4},{4,8},{8,12},{1,5},{5,9},{9,13},{2,6},{6,10},{10,14},{3,7},{... | collective-permute-start | bytes 18440 | tf_op jit(solution)/shard_map/ppermute | solution.py:15
  52.7 12.8 %copy-start.7 = (bf16[1,2,128]{2,1,0:T(2,128)(2,1)S(1)}, bf16[1,2,128]{2,1,0:T(2,128)(2,1)}, u32[]{:S(2)}) copy-start(bf16[1,2,128]{2,1,0:T(2,128)(2,1)} %param.23) | copy-start | bytes 1540
  52.7 12.8 %copy-start.11 = (bf16[1,2,128]{2,1,0:T(2,128)(2,1)S(1)}, bf16[1,2,128]{2,1,0:T(2,128)(2,1)}, u32[]{:S(2)}) copy-start(bf16[1,2,128]{2,1,0:T(2,128)(2,1)} %param.24) | copy-start | bytes 1540
  52.8 12.9 %copy-start.12 = (f32[1,2]{1,0:T(1,128)S(1)}, f32[1,2]{1,0:T(1,128)}, u32[]{:S(2)}) copy-start(f32[1,2]{1,0:T(1,128)} %param.27) | copy-start | bytes 28
  52.8 12.9 %copy-start.4 = (f32[1,2,1024]{2,1,0:T(2,128)S(1)}, f32[1,2,1024]{2,1,0:T(2,128)}, u32[]{:S(2)}) copy-start(f32[1,2,1024]{2,1,0:T(2,128)} %param.22) | copy-start | bytes 24580
  54.2 41.7 %copy-start.6 = (f32[1,2,1024]{2,1,0:T(2,128)S(1)}, f32[1,2,1024]{2,1,0:T(2,128)}, u32[]{:S(2)}) copy-start(f32[1,2,1024]{2,1,0:T(2,128)} %param.21) | copy-start | bytes 24580
  54.2 41.9 %copy-start.8 = (f32[1,2]{1,0:T(1,128)S(1)}, f32[1,2]{1,0:T(1,128)}, u32[]{:S(2)}) copy-start(f32[1,2]{1,0:T(1,128)} %param.26) | copy-start | bytes 28
  61.4 18.7 %all-to-all-start = ((bf16[1,8,256,128]{3,2,0,1:T(8,128)(2,1)}), bf16[1,8,256,128]{3,2,0,1:T(8,128)(2,1)}, u32[]{:S(2)}, u32[]{:S(2)}) async-start(bf16[1,8,256,128]{3,2,0,1:T(8,128)(2,1)} %fusion.30), calls=%async_computation | async-start | bytes 1048576 | tf_op jit(solution)/shard_map/all_to_all | solution.py:113
  80.1 12.3 %all-to-all-start.3 = ((bf16[4,2,256,128]{3,2,1,0:T(8,128)(2,1)}), bf16[4,2,256,128]{3,2,1,0:T(8,128)(2,1)S(1)}, u32[]{:S(2)}, u32[]{:S(2)}) async-start(bf16[4,2,256,128]{3,2,1,0:T(8,128)(2,1)} %bitcast.18), calls=%async_computation.3 | async-start | bytes 1048576 | tf_op jit(solution)/shard_map/all_to_all | solution.py:119
  92.3 13.7 %copy-start.9 = (bf16[1,2,128]{2,1,0:T(2,128)(2,1)S(1)}, bf16[1,2,128]{2,1,0:T(2,128)(2,1)}, u32[]{:S(2)}) copy-start(bf16[1,2,128]{2,1,0:T(2,128)(2,1)} %param.25) | copy-start | bytes 1540
  92.3 12.4 %all-to-all-start.1 = ((bf16[4,2,256,128]{3,2,1,0:T(8,128)(2,1)}), bf16[4,2,256,128]{3,2,1,0:T(8,128)(2,1)S(1)}, u32[]{:S(2)}, u32[]{:S(2)}) async-start(bf16[4,2,256,128]{3,2,1,0:T(8,128)(2,1)} %bitcast.10), calls=%async_computation.1 | async-start | bytes 1048576 | tf_op jit(solution)/shard_map/all_to_all | solution.py:112
  96.2 10.4 %copy-start.1 = (bf16[4,2,256,128]{3,2,0,1:T(8,128)(2,1)}, bf16[4,2,256,128]{3,2,0,1:T(8,128)(2,1)S(1)}, u32[]{:S(2)}) copy-start(bf16[4,2,256,128]{3,2,0,1:T(8,128)(2,1)S(1)} %copy.45) | copy-start | bytes 1572868
  104.8 1.9 %copy-start.2 = (bf16[4,2,256,128]{3,2,0,1:T(8,128)(2,1)}, bf16[4,2,256,128]{3,2,0,1:T(8,128)(2,1)S(1)}, u32[]{:S(2)}) copy-start(bf16[4,2,256,128]{3,2,0,1:T(8,128)(2,1)S(1)} %copy.42) | copy-start | bytes 1572868
where the time goes:
time: 107 us
  waiting for transfers between devices  48.4 us (45%)
  starting transfers between devices  33.8 us (32%)
  matrix products  10.3 us (10%)
  other arithmetic  9.68 us (9%)
  local copies, waits for them, and re-layouts  3.49 us (3%)
    all_to_all x1, waiting for transfers between devices, shards(): lax.all_to_all(keys, 'tp', split_axis=1, concat_axis=0, tiled=True)  11.6 us
    all_to_all x1, waiting for transfers between devices, shards(): lax.all_to_all(lax.all_to_all(values, 'tp', split_axis=1, concat_axis=0,...  8.61 us
    all_to_all x1, waiting for transfers between devices, shards(): lax.all_to_all(lax.all_to_all(keys, 'tp', split_axis=1, concat_axis=0, ti...  8.51 us
    all_to_all x1, waiting for transfers between devices, shards(): lax.all_to_all(values, 'tp', split_axis=1, concat_axis=0, tiled=True)  7.12 us
    all_to_all x1, starting transfers between devices, shards(): lax.all_to_all(forget_linear, 'tp', split_axis=1, concat_axis=0, tiled=True)  6.35 us
    all_to_all x1, waiting for transfers between devices, shards(): lax.all_to_all(input_linear, 'tp', split_axis=1, concat_axis=0, tiled=True)  4.89 us
    dot_general x1, matrix products, project_rows(): jnp.einsum('apd,dhk->ahpk', normed, value_matrix, preferred_element_type=...  4.29 us
    all_to_all x1, starting transfers between devices, shards(): lax.all_to_all(values, 'tp', split_axis=1, concat_axis=0, tiled=True)  4.14 us
  transfers between devices with their start and end apart: 9, of which 8 were waited for; matrix products, arithmetic and copies ran while one was open for 14% of the time, Pallas kernels for 0%

commit v1 on v0

--- a/solution.py
+++ b/solution.py
@@ -7,6 +7,22 @@
 DK = 128
 CONV = 4
 epsilon = 1e-06
+
+
+def pairwise_exchange(x, axis, split, join):
+    ways, here = (lax.axis_size(axis), lax.axis_index(axis))
+    width = x.shape[split] // ways
+    shape = list(x.shape)
+    shape[split] = width
+    height = shape[join]
+    shape[join] = height * ways
+    full = jnp.zeros(shape, x.dtype)
+    for mask in range(ways):
+        part = lax.dynamic_slice_in_dim(x, (here ^ mask) * width, width, axis=split)
+        if mask:
+            part = lax.ppermute(part, axis, [(d, d ^ mask) for d in range(ways)])
+        full = lax.dynamic_update_slice_in_dim(full, part, (here ^ mask) * height, axis=join)
+    return full
 
 
 def shifted(block, axis, distance):
@@ -124,7 +140,7 @@
             tiled=True,
         ),
         lax.all_to_all(
-            lax.all_to_all(input_linear, "tp", split_axis=1, concat_axis=0, tiled=True),
+            pairwise_exchange(input_linear, "tp", 1, 0),
             "sp",
             split_axis=0,
             concat_axis=2,

time: 107 us -> 104 us (0.972)
  waiting for transfers between devices: 48.4 us -> 42.7 us
  local copies, waits for them, and re-layouts: 3.49 us -> 5.1 us
  starting transfers between devices: 33.8 us -> 35.1 us
    ppermute x0 -> x3, starting transfers between devices: none -> 4.53 us  [pairwise_exchange(): part = lax.ppermute(part, axis, [(d, d ^ mask) for d in range(ways)])]
    all_to_all x1, waiting for transfers between devices: 3.82 us -> 0.01 us  [shards(): lax.all_to_all(forget_linear, 'tp', split_axis=1, concat_axis=0, tiled=True)]
    all_to_all x2 -> x1, starting transfers between devices: 6.49 us -> 3.25 us  [shards(): lax.all_to_all(pairwise_exchange(input_linear, 'tp', 1, 0), 'sp', split_a...]
    all_to_all x1, waiting for transfers between devices: 3.1 us -> 0.01 us  [shards(): lax.all_to_all(lax.all_to_all(forget_linear, 'tp', split_axis=1, concat_a...]
    ppermute x0 -> x3, waiting for transfers between devices: none -> 3 us  [pairwise_exchange(): part = lax.ppermute(part, axis, [(d, d ^ mask) for d in range(ways)])]
    all_to_all x1, waiting for transfers between devices: 8.61 us -> 5.78 us  [shards(): lax.all_to_all(lax.all_to_all(values, 'tp', split_axis=1, concat_axis=0,...]
    all_to_all x1, waiting for transfers between devices: 11.6 us -> 14.4 us  [shards(): lax.all_to_all(keys, 'tp', split_axis=1, concat_axis=0, tiled=True)]
    dynamic_update_slice x0 -> x4, local copies, waits for them, and re-layouts: none -> 2.26 us  [pairwise_exchange(): lax.dynamic_update_slice_in_dim(full, part, (here ^ mask) * height, axis=...]
  transfers between devices with their start and end apart: 9 -> 11, of which waited for: 8 -> 8; matrix products, arithmetic and copies ran while one was open for 14% -> 16% of each run, Pallas kernels for 0% -> 0%
where the time goes in v1:
time: 104 us; the launch traced here: 103 us
  waiting for transfers between devices  42.7 us (41%)
  starting transfers between devices  35.1 us (34%)
  matrix products  10.3 us (10%)
  other arithmetic  9 us (9%)
  local copies, waits for them, and re-layouts  5.1 us (5%)
    all_to_all x1, waiting for transfers between devices, shards(): lax.all_to_all(keys, 'tp', split_axis=1, concat_axis=0, tiled=True)  14.4 us
    all_to_all x1, waiting for transfers between devices, shards(): lax.all_to_all(lax.all_to_all(keys, 'tp', split_axis=1, concat_axis=0, ti...  8.51 us
    all_to_all x1, waiting for transfers between devices, shards(): lax.all_to_all(values, 'tp', split_axis=1, concat_axis=0, tiled=True)  7.11 us
    all_to_all x1, starting transfers between devices, shards(): lax.all_to_all(forget_linear, 'tp', split_axis=1, concat_axis=0, tiled=True)  6.35 us
    all_to_all x1, waiting for transfers between devices, shards(): lax.all_to_all(lax.all_to_all(values, 'tp', split_axis=1, concat_axis=0,...  5.78 us
    ppermute x3, starting transfers between devices, pairwise_exchange(): part = lax.ppermute(part, axis, [(d, d ^ mask) for d in range(ways)])  4.53 us
    dot_general x1, matrix products, project_rows(): jnp.einsum('apd,dhk->ahpk', normed, value_matrix, preferred_element_type=...  4.3 us
    all_to_all x1, starting transfers between devices, shards(): lax.all_to_all(keys, 'tp', split_axis=1, concat_axis=0, tiled=True)  4.14 us
  transfers between devices with their start and end apart: 11, of which 8 were waited for; matrix products, arithmetic and copies ran while one was open for 16% of the time, Pallas kernels for 0%

profile of v1, /device:TPU:0, one launch (start us, length us, event | category | flops | bytes accessed | tf_op | source)
XLA Modules:
  0.0 103.1 jit_solution(10686705724904647023)
XLA Ops:
  0.6 0.0 copy-start
  0.7 0.8 convert_element_type.127
  1.4 1.5 %fusion.6 = f32[256]{0:T(256)S(1)} fusion(bf16[1,256,2048]{2,1,0:T(8,128)(2,1)} %param.14), kind=kLoop, calls=%fused_computation.8 | loop fusion | flops 1572608 | bytes 1049600 | tf_op jit(solution)/shard_map/reduce_sum | solution.py:40
  3.0 1.7 %fusion.21 = bf16[1,8,256]{2,1,0:T(8,128)(2,1)S(1)} fusion(bf16[2048,8]{0,1:T(8,128)(2,1)S(1)} %copy-done, bf16[1,256,2048]{2,1,0:T(8,128)(2,1)} %param.14, f32[2048]{0:T(1024)S(1)} %convert_element_type.127, f32[256]{0:T(256)S(1)} %add_rsqrt_fusion), kind=kOutput, calls=%fused_computation.17 | convolution fusion | flops 10487808 | bytes 1094656 | tf_op jit(solution)/shard_map/apd,dh->ahp/dot_general | solution.py:54
  4.7 0.5 broadcast.49
  5.2 0.7 reduce.8
  5.9 0.6 reshape.225
  6.5 6.3 %all-to-all-start.5 = ((bf16[4,2,256]{2,1,0:T(2,128)(2,1)}), bf16[4,2,256]{2,1,0:T(2,128)(2,1)S(1)}, u32[]{:S(2)}, u32[]{:S(2)}) async-start(bf16[4,2,256]{2,1,0:T(2,128)(2,1)} %reshape.225), calls=%async_computation.5 | async-start | bytes 8192 | tf_op jit(solution)/shard_map/all_to_all | solution.py:150
  12.8 0.4 convolution_convert_fusion.1
  13.3 2.1 %collective-permute-start.1 = (bf16[1,2,256]{2,1,0:T(2,128)(2,1)S(1)}, bf16[1,2,256]{2,1,0:T(2,128)(2,1)S(1)}, u32[]{:S(2)}, u32[]{:S(2)}) collective-permute-start(bf16[1,2,256]{2,1,0:T(2,128)(2,1)S(1)} %get-tuple-element.17), channel_id=1, source_target_pairs={{0,1},{1,0},{2,3},{3,2},{4,5},{5,4},{6,7},{7,6},{8,9},{9,8},{10,11... | collective-permute-start | bytes 3080 | tf_op jit(solution)/shard_map/ppermute | solution.py:23
  15.4 2.4 %collective-permute-start.2 = (bf16[1,2,256]{2,1,0:T(2,128)(2,1)S(1)}, bf16[1,2,256]{2,1,0:T(2,128)(2,1)S(1)}, u32[]{:S(2)}, u32[]{:S(2)}) collective-permute-start(bf16[1,2,256]{2,1,0:T(2,128)(2,1)S(1)} %get-tuple-element.16), channel_id=1, source_target_pairs={{0,2},{1,3},{2,0},{3,1},{4,6},{5,7},{6,4},{7,5},{8,10},{9,11},{10,... | collective-permute-start | bytes 3080 | tf_op jit(solution)/shard_map/ppermute | solution.py:23
  17.7 0.1 collective-permute-start.3
  17.8 0.6 broadcast_in_dim.2
  18.4 0.6 constant_dynamic-update-slice_fusion.3
  19.0 0.6 constant_dynamic-update-slice_fusion.2
  19.6 0.3 collective-permute-done.2
  19.9 0.6 constant_dynamic-update-slice_fusion.1
  20.4 2.7 %collective-permute-done.3 = bf16[1,2,256]{2,1,0:T(2,128)(2,1)S(1)} collective-permute-done((bf16[1,2,256]{2,1,0:T(2,128)(2,1)S(1)}, bf16[1,2,256]{2,1,0:T(2,128)(2,1)S(1)}, u32[]{:S(2)}, u32[]{:S(2)}) %collective-permute-start.3) | collective-permute-done | bytes 1056 | tf_op jit(solution)/shard_map/ppermute | solution.py:23
  23.1 0.6 constant_dynamic-update-slice_fusion
  23.7 3.2 %all-to-all-start.4 = ((bf16[4,2,256]{2,1,0:T(2,128)(2,1)}), bf16[4,2,256]{2,1,0:T(2,128)(2,1)S(1)}, u32[]{:S(2)}, u32[]{:S(2)}) async-start(bf16[4,2,256]{2,1,0:T(2,128)(2,1)} %constant_dynamic-update-slice_fusion), calls=%async_computation.4 | async-start | bytes 8192 | tf_op jit(solution)/shard_map/all_to_all | solution.py:142
  27.0 0.6 all_to_all.81
  27.6 3.1 %all-to-all-done.4 = bf16[4,2,256]{2,1,0:T(2,128)(2,1)S(1)} async-done(((bf16[4,2,256]{2,1,0:T(2,128)(2,1)}), bf16[4,2,256]{2,1,0:T(2,128)(2,1)S(1)}, u32[]{:S(2)}, u32[]{:S(2)}) %all-to-all-start.4) | async-done | bytes 4128 | tf_op jit(solution)/shard_map/all_to_all | solution.py:142
  30.7 3.2 %all-to-all-start.6 = ((bf16[4,2,256]{2,1,0:T(2,128)(2,1)}), bf16[4,2,256]{2,1,0:T(2,128)(2,1)S(1)}, u32[]{:S(2)}, u32[]{:S(2)}) async-start(bf16[4,2,256]{2,1,0:T(2,128)(2,1)} %all_to_all.81), calls=%async_computation.6 | async-start | bytes 8192 | tf_op jit(solution)/shard_map/all_to_all | solution.py:149
  34.0 4.3 %fusion.15 = bf16[1,8,256,128]{3,2,0,1:T(8,128)(2,1)} fusion(bf16[1,256,2048]{2,1,0:T(8,128)(2,1)S(1)} %copy-done.3, f32[2048]{0:T(1024)S(1)} %convert_element_type.127, f32[256]{0:T(256)S(1)} %add_rsqrt_fusion, bf16[2048,1024]{1,0:T(8,128)(2,1)} %param.17), kind=kOutput, calls=%fused_computation.13 | convolution fusion | flops 1076101120 | bytes 5776384 | tf_op jit(solution)/shard_map/apd,dhk->ahpk/dot_general | solution.py:48
  38.3 4.1 %all-to-all-start.2 = ((bf16[1,8,256,128]{3,2,0,1:T(8,128)(2,1)}), bf16[1,8,256,128]{3,2,0,1:T(8,128)(2,1)}, u32[]{:S(2)}, u32[]{:S(2)}) async-start(bf16[1,8,256,128]{3,2,0,1:T(8,128)(2,1)} %fusion.15), calls=%async_computation.2 | async-start | bytes 1048576 | tf_op jit(solution)/shard_map/all_to_all | solution.py:136
  42.4 3.5 %fusion.18 = bf16[1,8,256,128]{3,2,1,0:T(8,128)(2,1)S(1)} fusion(bf16[1,256,2048]{2,1,0:T(8,128)(2,1)S(1)} %copy-done.3, f32[2048]{0:T(1024)S(1)} %convert_element_type.127, f32[256]{0:T(256)S(1)} %add_rsqrt_fusion, bf16[2048,1024]{1,0:T(8,128)(2,1)} %param.16), kind=kOutput, calls=%fused_computation.14 | convolution fusion | flops 1076101120 | bytes 5776384 | tf_op jit(solution)/shard_map/apd,dhk->ahpk/dot_general | solution.py:45
  45.9 2.4 %collective-permute-start = (bf16[1,8,3,128]{3,2,1,0:T(4,128)(2,1)S(1)}, bf16[1,8,3,128]{3,2,1,0:T(4,128)(2,1)S(1)}, u32[]{:S(2)}, u32[]{:S(2)}) collective-permute-start(bf16[1,8,3,128]{3,2,1,0:T(4,128)(2,1)S(1)} %slice.48), channel_id=1, source_target_pairs={{0,4},{4,8},{8,12},{1,5},{5,9},{9,13},{2,6},{6,10},{10,14},{3,7},{... | collective-permute-start | bytes 18440 | tf_op jit(solution)/shard_map/ppermute | solution.py:31
  48.3 0.8 collective-permute-done
  49.1 0.1 maximum_convert_fusion
  49.3 1.5 %fusion.29 = bf16[1,8,256,128]{3,2,0,1:T(8,128)(2,1)} fusion(f32[8,128]{1,0:T(8,128)S(1)} %bitcast.180, f32[1,8,259,128]{3,2,1,0:T(8,128)S(1)} %maximum_convert_fusion, f32[8,128]{1,0:T(8,128)S(1)} %bitcast.181, f32[8,128]{1,0:T(8,128)S(1)} %bitcast.179, f32[8,128]{1,0:T(8,128)S(1)} %bitcast.178), kind=kLoop, calls=%fused_computation.31 | loop fusion | flops 3145728 | bytes 4734976 | tf_op jit(solution)/shard_map/convert_element_type | solution.py:67
  50.7 7.1 %all-to-all-done.2 = bf16[1,8,256,128]{3,2,0,1:T(8,128)(2,1)} async-done(((bf16[1,8,256,128]{3,2,0,1:T(8,128)(2,1)}), bf16[1,8,256,128]{3,2,0,1:T(8,128)(2,1)}, u32[]{:S(2)}, u32[]{:S(2)}) %all-to-all-start.2) | async-done | bytes 524320 | tf_op jit(solution)/shard_map/all_to_all | solution.py:136
  57.8 4.1 %all-to-all-start = ((bf16[1,8,256,128]{3,2,0,1:T(8,128)(2,1)}), bf16[1,8,256,128]{3,2,0,1:T(8,128)(2,1)}, u32[]{:S(2)}, u32[]{:S(2)}) async-start(bf16[1,8,256,128]{3,2,0,1:T(8,128)(2,1)} %fusion.29), calls=%async_computation | async-start | bytes 1048576 | tf_op jit(solution)/shard_map/all_to_all | solution.py:129
  62.0 0.1 multiply_reduce_fusion
  62.2 14.4 %all-to-all-done = bf16[1,8,256,128]{3,2,0,1:T(8,128)(2,1)} async-done(((bf16[1,8,256,128]{3,2,0,1:T(8,128)(2,1)}), bf16[1,8,256,128]{3,2,0,1:T(8,128)(2,1)}, u32[]{:S(2)}, u32[]{:S(2)}) %all-to-all-start) | async-done | bytes 524320 | tf_op jit(solution)/shard_map/all_to_all | solution.py:129
  76.6 3.5 %all-to-all-start.3 = ((bf16[4,2,256,128]{3,2,1,0:T(8,128)(2,1)}), bf16[4,2,256,128]{3,2,1,0:T(8,128)(2,1)S(1)}, u32[]{:S(2)}, u32[]{:S(2)}) async-start(bf16[4,2,256,128]{3,2,1,0:T(8,128)(2,1)} %bitcast.18), calls=%async_computation.3 | async-start | bytes 1048576 | tf_op jit(solution)/shard_map/all_to_all | solution.py:135
  80.1 2.5 %reduce-window.6 = f32[1,2,8,128]{3,2,1,0:T(8,128)S(1)} reduce-window(f32[1,2,8,128]{3,2,1,0:T(8,128)S(1)} %copy.75, f32[]{:T(128)} %constant.14.clone.1), window={size=1x1x1x128 pad=0_0x0_0x0_0x0_127}, to_apply=%region_1.2 | reduce-window | flops 260096 | bytes 16388 | tf_op jit(solution)/shard_map/reduce-window
  82.6 0.1 slice_reduce_fusion
  82.7 0.2 reduce-window.9
  82.9 0.1 slice_bitcast_fusion
  83.0 0.1 broadcast.41
  83.1 5.8 %all-to-all-done.3 = bf16[4,2,256,128]{3,2,1,0:T(8,128)(2,1)S(1)} async-done(((bf16[4,2,256,128]{3,2,1,0:T(8,128)(2,1)}), bf16[4,2,256,128]{3,2,1,0:T(8,128)(2,1)S(1)}, u32[]{:S(2)}, u32[]{:S(2)}) %all-to-all-start.3) | async-done | bytes 524320 | tf_op jit(solution)/shard_map/all_to_all | solution.py:135
  88.8 3.6 %all-to-all-start.1 = ((bf16[4,2,256,128]{3,2,1,0:T(8,128)(2,1)}), bf16[4,2,256,128]{3,2,1,0:T(8,128)(2,1)S(1)}, u32[]{:S(2)}, u32[]{:S(2)}) async-start(bf16[4,2,256,128]{3,2,1,0:T(8,128)(2,1)} %bitcast.10), calls=%async_computation.1 | async-start | bytes 1048576 | tf_op jit(solution)/shard_map/all_to_all | solution.py:128
  92.4 0.2 fusion.58
  92.7 8.5 %all-to-all-done.1 = bf16[4,2,256,128]{3,2,1,0:T(8,128)(2,1)S(1)} async-done(((bf16[4,2,256,128]{3,2,1,0:T(8,128)(2,1)}), bf16[4,2,256,128]{3,2,1,0:T(8,128)(2,1)S(1)}, u32[]{:S(2)}, u32[]{:S(2)}) %all-to-all-start.1) | async-done | bytes 524320 | tf_op jit(solution)/shard_map/all_to_all | solution.py:128
  101.3 0.2 fusion.39
  101.5 0.8 convert_reduce_fusion
  102.3 0.2 fusion.33
  102.5 0.6 fusion.41
  (46 shorter events, 0.4 us)
Async XLA Ops:
  0.6 2.3 %copy-start = (bf16[2048,8]{0,1:T(8,128)(2,1)S(1)}, bf16[2048,8]{0,1:T(8,128)(2,1)}, u32[]{:S(2)}) copy-start(bf16[2048,8]{0,1:T(8,128)(2,1)} %param.19) | copy-start | bytes 98308
  0.6 12.2 %copy-start.3 = (bf16[1,256,2048]{2,1,0:T(8,128)(2,1)S(1)}, bf16[1,256,2048]{2,1,0:T(8,128)(2,1)}, u32[]{:S(2)}) copy-start(bf16[1,256,2048]{2,1,0:T(8,128)(2,1)} %param.14) | copy-start | bytes 3145732
  0.7 12.2 %copy-start.10 = (bf16[2048,8]{0,1:T(8,128)(2,1)S(1)}, bf16[2048,8]{0,1:T(8,128)(2,1)}, u32[]{:S(2)}) copy-start(bf16[2048,8]{0,1:T(8,128)(2,1)} %param.18) | copy-start | bytes 98308
  6.5 17.2 %all-to-all-start.5 = ((bf16[4,2,256]{2,1,0:T(2,128)(2,1)}), bf16[4,2,256]{2,1,0:T(2,128)(2,1)S(1)}, u32[]{:S(2)}, u32[]{:S(2)}) async-start(bf16[4,2,256]{2,1,0:T(2,128)(2,1)} %reshape.225), calls=%async_computation.5 | async-start | bytes 8192 | tf_op jit(solution)/shard_map/all_to_all | solution.py:150
  13.3 5.7 %collective-permute-start.1 = (bf16[1,2,256]{2,1,0:T(2,128)(2,1)S(1)}, bf16[1,2,256]{2,1,0:T(2,128)(2,1)S(1)}, u32[]{:S(2)}, u32[]{:S(2)}) collective-permute-start(bf16[1,2,256]{2,1,0:T(2,128)(2,1)S(1)} %get-tuple-element.17), channel_id=1, source_target_pairs={{0,1},{1,0},{2,3},{3,2},{4,5},{5,4},{6,7},{7,6},{8,9},{9,8},{10,11... | collective-permute-start | bytes 3080 | tf_op jit(solution)/shard_map/ppermute | solution.py:23
  15.4 4.5 %collective-permute-start.2 = (bf16[1,2,256]{2,1,0:T(2,128)(2,1)S(1)}, bf16[1,2,256]{2,1,0:T(2,128)(2,1)S(1)}, u32[]{:S(2)}, u32[]{:S(2)}) collective-permute-start(bf16[1,2,256]{2,1,0:T(2,128)(2,1)S(1)} %get-tuple-element.16), channel_id=1, source_target_pairs={{0,2},{1,3},{2,0},{3,1},{4,6},{5,7},{6,4},{7,5},{8,10},{9,11},{10,... | collective-permute-start | bytes 3080 | tf_op jit(solution)/shard_map/ppermute | solution.py:23
  17.7 5.4 %collective-permute-start.3 = (bf16[1,2,256]{2,1,0:T(2,128)(2,1)S(1)}, bf16[1,2,256]{2,1,0:T(2,128)(2,1)S(1)}, u32[]{:S(2)}, u32[]{:S(2)}) collective-permute-start(bf16[1,2,256]{2,1,0:T(2,128)(2,1)S(1)} %get-tuple-element.15), channel_id=1, source_target_pairs={{0,3},{1,2},{2,1},{3,0},{4,7},{5,6},{6,5},{7,4},{8,11},{9,10},{10,... | collective-permute-start | bytes 3080 | tf_op jit(solution)/shard_map/ppermute | solution.py:23
  23.7 7.0 %all-to-all-start.4 = ((bf16[4,2,256]{2,1,0:T(2,128)(2,1)}), bf16[4,2,256]{2,1,0:T(2,128)(2,1)S(1)}, u32[]{:S(2)}, u32[]{:S(2)}) async-start(bf16[4,2,256]{2,1,0:T(2,128)(2,1)} %constant_dynamic-update-slice_fusion), calls=%async_computation.4 | async-start | bytes 8192 | tf_op jit(solution)/shard_map/all_to_all | solution.py:142
  30.7 7.6 %all-to-all-start.6 = ((bf16[4,2,256]{2,1,0:T(2,128)(2,1)}), bf16[4,2,256]{2,1,0:T(2,128)(2,1)S(1)}, u32[]{:S(2)}, u32[]{:S(2)}) async-start(bf16[4,2,256]{2,1,0:T(2,128)(2,1)} %all_to_all.81), calls=%async_computation.6 | async-start | bytes 8192 | tf_op jit(solution)/shard_map/all_to_all | solution.py:149
  38.3 19.6 %all-to-all-start.2 = ((bf16[1,8,256,128]{3,2,0,1:T(8,128)(2,1)}), bf16[1,8,256,128]{3,2,0,1:T(8,128)(2,1)}, u32[]{:S(2)}, u32[]{:S(2)}) async-start(bf16[1,8,256,128]{3,2,0,1:T(8,128)(2,1)} %fusion.15), calls=%async_computation.2 | async-start | bytes 1048576 | tf_op jit(solution)/shard_map/all_to_all | solution.py:136
  42.4 5.9 %copy-start.5 = (f32[4,1024]{1,0:T(4,128)S(1)}, f32[4,1024]{1,0:T(4,128)}, u32[]{:S(2)}) copy-start(f32[4,1024]{1,0:T(4,128)} %param.20) | copy-start | bytes 49156
  45.9 3.2 %collective-permute-start = (bf16[1,8,3,128]{3,2,1,0:T(4,128)(2,1)S(1)}, bf16[1,8,3,128]{3,2,1,0:T(4,128)(2,1)S(1)}, u32[]{:S(2)}, u32[]{:S(2)}) collective-permute-start(bf16[1,8,3,128]{3,2,1,0:T(4,128)(2,1)S(1)} %slice.48), channel_id=1, source_target_pairs={{0,4},{4,8},{8,12},{1,5},{5,9},{9,13},{2,6},{6,10},{10,14},{3,7},{... | collective-permute-start | bytes 18440 | tf_op jit(solution)/shard_map/ppermute | solution.py:31
  49.2 12.8 %copy-start.7 = (bf16[1,2,128]{2,1,0:T(2,128)(2,1)S(1)}, bf16[1,2,128]{2,1,0:T(2,128)(2,1)}, u32[]{:S(2)}) copy-start(bf16[1,2,128]{2,1,0:T(2,128)(2,1)} %param.23) | copy-start | bytes 1540
  49.2 12.8 %copy-start.11 = (bf16[1,2,128]{2,1,0:T(2,128)(2,1)S(1)}, bf16[1,2,128]{2,1,0:T(2,128)(2,1)}, u32[]{:S(2)}) copy-start(bf16[1,2,128]{2,1,0:T(2,128)(2,1)} %param.24) | copy-start | bytes 1540
  49.2 12.9 %copy-start.12 = (f32[1,2]{1,0:T(1,128)S(1)}, f32[1,2]{1,0:T(1,128)}, u32[]{:S(2)}) copy-start(f32[1,2]{1,0:T(1,128)} %param.27) | copy-start | bytes 28
  50.7 29.3 %copy-start.4 = (f32[1,2,1024]{2,1,0:T(2,128)S(1)}, f32[1,2,1024]{2,1,0:T(2,128)}, u32[]{:S(2)}) copy-start(f32[1,2,1024]{2,1,0:T(2,128)} %param.22) | copy-start | bytes 24580
  50.7 41.7 %copy-start.6 = (f32[1,2,1024]{2,1,0:T(2,128)S(1)}, f32[1,2,1024]{2,1,0:T(2,128)}, u32[]{:S(2)}) copy-start(f32[1,2,1024]{2,1,0:T(2,128)} %param.21) | copy-start | bytes 24580
  50.7 41.9 %copy-start.8 = (f32[1,2]{1,0:T(1,128)S(1)}, f32[1,2]{1,0:T(1,128)}, u32[]{:S(2)}) copy-start(f32[1,2]{1,0:T(1,128)} %param.26) | copy-start | bytes 28
  57.8 18.7 %all-to-all-start = ((bf16[1,8,256,128]{3,2,0,1:T(8,128)(2,1)}), bf16[1,8,256,128]{3,2,0,1:T(8,128)(2,1)}, u32[]{:S(2)}, u32[]{:S(2)}) async-start(bf16[1,8,256,128]{3,2,0,1:T(8,128)(2,1)} %fusion.29), calls=%async_computation | async-start | bytes 1048576 | tf_op jit(solution)/shard_map/all_to_all | solution.py:129
  76.6 12.3 %all-to-all-start.3 = ((bf16[4,2,256,128]{3,2,1,0:T(8,128)(2,1)}), bf16[4,2,256,128]{3,2,1,0:T(8,128)(2,1)S(1)}, u32[]{:S(2)}, u32[]{:S(2)}) async-start(bf16[4,2,256,128]{3,2,1,0:T(8,128)(2,1)} %bitcast.18), calls=%async_computation.3 | async-start | bytes 1048576 | tf_op jit(solution)/shard_map/all_to_all | solution.py:135
  88.8 13.7 %copy-start.9 = (bf16[1,2,128]{2,1,0:T(2,128)(2,1)S(1)}, bf16[1,2,128]{2,1,0:T(2,128)(2,1)}, u32[]{:S(2)}) copy-start(bf16[1,2,128]{2,1,0:T(2,128)(2,1)} %param.25) | copy-start | bytes 1540
  88.8 12.4 %all-to-all-start.1 = ((bf16[4,2,256,128]{3,2,1,0:T(8,128)(2,1)}), bf16[4,2,256,128]{3,2,1,0:T(8,128)(2,1)S(1)}, u32[]{:S(2)}, u32[]{:S(2)}) async-start(bf16[4,2,256,128]{3,2,1,0:T(8,128)(2,1)} %bitcast.10), calls=%async_computation.1 | async-start | bytes 1048576 | tf_op jit(solution)/shard_map/all_to_all | solution.py:128
  92.7 10.4 %copy-start.1 = (bf16[4,2,256,128]{3,2,0,1:T(8,128)(2,1)}, bf16[4,2,256,128]{3,2,0,1:T(8,128)(2,1)S(1)}, u32[]{:S(2)}) copy-start(bf16[4,2,256,128]{3,2,0,1:T(8,128)(2,1)S(1)} %copy.41) | copy-start | bytes 1572868
  101.3 1.9 %copy-start.2 = (bf16[4,2,256,128]{3,2,0,1:T(8,128)(2,1)}, bf16[4,2,256,128]{3,2,0,1:T(8,128)(2,1)S(1)}, u32[]{:S(2)}) copy-start(bf16[4,2,256,128]{3,2,0,1:T(8,128)(2,1)S(1)} %copy.38) | copy-start | bytes 1572868
